TPU v7x, 32 devices: a whole 2x2x4 slice. The times are simulated.
32 devices in a mesh: gr: 2 (over x), sp: 8 (over z, y), tp: 2 (over core).
Axes of the slice: x: 2, y: 2, z: 4, core: 2. Of those that a mesh axis runs over, the one named last changes fastest.
Arguments:
- tokens: bfloat16 [16, 512, 4096], P('gr', 'sp'), may hold values from -6 to 6
- key_weight: bfloat16 [4096, 2048], P(('gr', 'sp'), 'tp'), may hold values from -0.09375 to 0.09375
- value_weight: bfloat16 [4096, 2048], P(('gr', 'sp'), 'tp'), may hold values from -0.09375 to 0.09375
- gate_weight: bfloat16 [4096, 16], P(('gr', 'sp'), 'tp'), may hold values from -0.09375 to 0.09375
- forget_bias: float32 [16], P('tp'), may hold values from 7 to 9
- new_query: bfloat16 [16, 16, 128], P('gr', 'tp'), may hold values from -6 to 6
Outputs:
- key_cache: bfloat16 [16, 16, 512, 128], P(('gr', 'sp'), 'tp')
- value_cache: bfloat16 [16, 16, 512, 128], P(('gr', 'sp'), 'tp')
- gate_cache: float32 [16, 16, 512], P(('gr', 'sp'), 'tp')
- first_read: bfloat16 [16, 16, 128], P(('gr', 'sp'), 'tp')
All inputs are finite; a program needn't handle non-finite values.
Results may differ from a plain program's by a relative error of at most 0.0075.
Values may be sent and summed in bfloat16 or wider, within the bound.
A program may use at most 64 MiB of HBM per device.

v0:
```python
import jax
import jax.numpy as jnp
from jax import lax
from jax.sharding import PartitionSpec as P

eps = 1e-06


def taken_in(piece, axis, dim, turn, start):

    def gathered(part):
        return lax.all_gather(part, axis, axis=dim, tiled=True)

    return turn(start, jax.tree.map(gathered, piece), jnp.int32(0))


def carried_in(array, axis, combine, identity, reverse):
    length, mine = (lax.axis_size(axis), lax.axis_index(axis))
    everything = jax.tree.map(lambda part: lax.all_gather(part, axis), array)
    start = jax.tree.map(
        lambda part, zero: jnp.broadcast_to(jnp.asarray(zero, part.dtype), part.shape),
        array,
        identity,
    )

    def turn(k, before):
        at = length - 1 - k if reverse else k
        reached = at > mine if reverse else at < mine
        new = combine(before, jax.tree.map(lambda part: part[at], everything))
        return jax.tree.map(lambda a, b: jnp.where(reached, a, b), new, before)

    return lax.fori_loop(0, length, turn, start)


def add_pair(earlier, later):
    return earlier + later


def partial_read(queries, keys, values, cumulative, scaling):
    scores = (
        jnp.einsum("shd,shpd->shp", queries, keys, preferred_element_type=jnp.float32) * scaling
        - cumulative
    )
    highest = jnp.max(scores, axis=2)
    weights = jnp.exp(scores - highest[..., None])
    weight_sum = jnp.sum(weights, axis=2)
    value_sum = jnp.einsum("shp,shpd->shd", weights, values.astype(jnp.float32))
    return (highest, weight_sum, value_sum)


def on_device(tokens, key_weight, value_weight, gate_weight, forget_bias, new_query):
    sequences, positions, features = tokens.shape
    heads_here = forget_bias.shape[0]
    head_dim = new_query.shape[2]
    scaling = head_dim ** (-0.5)
    row_count = sequences * positions
    flat = tokens.reshape(row_count, features)
    empty_kv = jnp.zeros((row_count, key_weight.shape[1]), jnp.float32)
    empty_gate = jnp.zeros((row_count, heads_here), jnp.float32)
    initial = (empty_kv, empty_kv, empty_gate)

    def add_rows(sums, pieces, start):
        columns = lax.dynamic_slice_in_dim(flat, start, pieces[0].shape[0], 1)
        return tuple(
            (
                running + jnp.dot(columns, piece, preferred_element_type=jnp.float32)
                for running, piece in zip(sums, pieces)
            )
        )

    projected = taken_in(
        (key_weight, value_weight, gate_weight), ("gr", "sp"), 0, add_rows, initial
    )
    key_sum, value_sum, gate_logit = projected
    keys = (
        key_sum.astype(jnp.bfloat16)
        .reshape(sequences, positions, heads_here, head_dim)
        .transpose(0, 2, 1, 3)
    )
    values = (
        value_sum.astype(jnp.bfloat16)
        .reshape(sequences, positions, heads_here, head_dim)
        .transpose(0, 2, 1, 3)
    )
    log_gate = jax.nn.log_sigmoid(gate_logit + forget_bias).reshape(
        sequences, positions, heads_here
    )
    running_gate = jnp.cumsum(log_gate.transpose(0, 2, 1), axis=2)
    earlier_sum = carried_in(
        running_gate[:, :, -1],
        "sp",
        add_pair,
        jnp.zeros((sequences, heads_here), jnp.float32),
        False,
    )
    cumulative = running_gate + earlier_sum[:, :, None]
    key_cache, value_cache = (
        lax.all_to_all(keys, "sp", split_axis=0, concat_axis=2, tiled=True),
        lax.all_to_all(values, "sp", split_axis=0, concat_axis=2, tiled=True),
    )
    gate_cache = lax.all_to_all(cumulative, "sp", split_axis=0, concat_axis=2, tiled=True)
    member = lax.axis_index("sp")
    own_query = lax.dynamic_slice_in_dim(new_query, member, 1, 0)
    highest, weight_sum, value_total = partial_read(
        own_query, key_cache, value_cache, gate_cache, scaling
    )
    attended = value_total / weight_sum[..., None]
    normed = attended * lax.rsqrt(jnp.mean(attended * attended, axis=-1, keepdims=True) + eps)
    return (key_cache, value_cache, gate_cache, normed.astype(jnp.bfloat16))


def solution(mesh):
    in_specs = (
        P("gr", "sp", None),
        P(("gr", "sp"), "tp"),
        P(("gr", "sp"), "tp"),
        P(("gr", "sp"), "tp"),
        P("tp"),
        P("gr", "tp", None),
    )
    out_specs = (
        P(("gr", "sp"), "tp", None, None),
        P(("gr", "sp"), "tp", None, None),
        P(("gr", "sp"), "tp", None),
        P(("gr", "sp"), "tp", None),
    )
    return jax.shard_map(
        on_device, mesh=mesh, in_specs=in_specs, out_specs=out_specs, check_vma=False
    )
```

profile of v0, /device:TPU:0, one launch (start us, length us, event | category | flops | bytes accessed | tf_op | source)
XLA Modules:
  0.0 302.6 jit_solution(3733088857924785863)
XLA Ops:
  7.2 0.0 copy-start
  7.2 0.0 all-gather.4.cloned.1.call-start
  7.2 0.7 all-gather.4.cloned.1.call-update
  7.9 0.0 all-gather.6.cloned.1.call-start
  8.0 0.7 all-gather.6.cloned.1.call-update
  8.7 44.0 %all_gather.14 = bf16[4096,8]{0,1:T(8,128)(2,1)S(1)} all-gather(bf16[256,8]{0,1:T(8,128)(2,1)} %param.11), channel_id=1, replica_groups=mesh['gr'=2,'sp'=8,'tp'=2] {'gr','sp'}, dimensions={0}, use_global_device_ids=true | all-gather | bytes 69632 | tf_op jit(solution)/shard_map/all_gather | solution.py:12
  52.7 3.4 %fusion.7 = f32[512,8]{0,1:T(8,128)S(1)} fusion(bf16[512,4096]{1,0:T(8,128)(2,1)} %bitcast.73, bf16[4096,8]{0,1:T(8,128)(2,1)S(1)} %all_gather.14, f32[8]{0:T(128)} %param.12), kind=kOutput, calls=%fused_computation.15 | convolution fusion | flops 33591296 | bytes 4276256 | tf_op jit(solution)/shard_map/dot_general | solution.py:66
  56.1 0.1 reshape.72
  56.2 1.8 reduce_window_sum.11
  57.9 0.1 slice.4
  58.0 0.1 copy.23
  58.1 31.4 %all-gather = f32[64,8,1]{1,2,0:T(1,128)S(1)} all-gather(f32[8,8,1]{1,2,0:T(1,128)S(1)} %copy.23), channel_id=2, replica_groups=mesh['gr'=2,'sp'=8,'tp'=2] {'sp'}, dimensions={0}, use_global_device_ids=true | all-gather | bytes 2304 | tf_op jit(solution)/shard_map/all_gather | solution.py:19
  89.6 0.2 while.14
  89.8 0.1 broadcast_add_fusion
  89.9 0.7 reshape.81
  90.6 3.3 %all-to-all-start.2 = ((f32[8,1,512]{2,1,0:T(1,128)}), f32[8,1,512]{2,1,0:T(1,128)S(1)}, u32[]{:S(2)}, u32[]{:S(2)}) async-start(f32[8,1,512]{2,1,0:T(1,128)} %reshape.81), calls=%async_computation.2 | async-start | bytes 32768 | tf_op jit(solution)/shard_map/all_to_all | solution.py:101
  93.9 32.5 %all-gather.4.cloned.1.call-done = bf16[4096,1024]{1,0:T(8,128)(2,1)} async-done(((bf16[256,1024]{1,0:T(8,128)(2,1)}), bf16[4096,1024]{1,0:T(8,128)(2,1)}) %all-gather.4.cloned.1.call-update) | async-done | bytes 8388624 | tf_op jit(solution)/shard_map/all_gather | solution.py:12
  126.4 9.1 %fusion = bf16[64,8,8,128]{3,1,2,0:T(8,128)(2,1)S(1)} fusion(bf16[512,4096]{1,0:T(8,128)(2,1)} %bitcast.74, bf16[4096,1024]{1,0:T(8,128)(2,1)} %all-gather.4.cloned.1.call-done), kind=kOutput, calls=%fused_computation.3 | convolution fusion | flops 4295491584 | bytes 13631488 | tf_op jit(solution)/shard_map/dot_general | solution.py:66
  135.6 0.3 copy.35
  135.8 1.0 bitcast_bitcast_fusion.1
  136.9 0.0 all-to-all-done.2
  136.9 3.7 %all-to-all-start = ((bf16[8,8,64,128]{3,1,2,0:T(8,128)(2,1)}), bf16[8,8,64,128]{3,1,2,0:T(8,128)(2,1)S(1)}, u32[]{:S(2)}, u32[]{:S(2)}) async-start(bf16[8,8,64,128]{3,1,2,0:T(8,128)(2,1)} %bitcast_bitcast_fusion.1), calls=%async_computation | async-start | bytes 2097152 | tf_op jit(solution)/shard_map/all_to_all | solution.py:98
  140.6 111.7 %all-gather.6.cloned.1.call-done = bf16[4096,1024]{1,0:T(8,128)(2,1)} async-done(((bf16[256,1024]{1,0:T(8,128)(2,1)}), bf16[4096,1024]{1,0:T(8,128)(2,1)}) %all-gather.6.cloned.1.call-update) | async-done | bytes 8388624 | tf_op jit(solution)/shard_map/all_gather | solution.py:12
  252.2 9.1 %fusion.1 = bf16[64,8,8,128]{3,1,2,0:T(8,128)(2,1)S(1)} fusion(bf16[512,4096]{1,0:T(8,128)(2,1)} %bitcast.75, bf16[4096,1024]{1,0:T(8,128)(2,1)} %all-gather.6.cloned.1.call-done), kind=kOutput, calls=%fused_computation.4 | convolution fusion | flops 4295491584 | bytes 13631488 | tf_op jit(solution)/shard_map/dot_general | solution.py:66
  261.4 0.3 copy.36
  261.6 1.0 bitcast_bitcast_fusion
  262.7 0.0 all-to-all-done
  262.7 3.7 %all-to-all-start.1 = ((bf16[8,8,64,128]{3,1,2,0:T(8,128)(2,1)}), bf16[8,8,64,128]{3,1,2,0:T(8,128)(2,1)S(1)}, u32[]{:S(2)}, u32[]{:S(2)}) async-start(bf16[8,8,64,128]{3,1,2,0:T(8,128)(2,1)} %bitcast_bitcast_fusion), calls=%async_computation.1 | async-start | bytes 2097152 | tf_op jit(solution)/shard_map/all_to_all | solution.py:99
  266.4 0.0 copy-done
  266.4 0.5 broadcast.38
  266.9 0.7 reduce.6
  267.6 0.1 reshape.82
  267.7 0.1 all_to_all.53
  267.8 0.7 all_to_all.52
  268.5 0.4 fusion.5
  268.8 0.1 fusion.14
  269.0 0.2 fusion.10
  269.2 0.1 fusion.11
  269.2 22.9 %all-to-all-done.1 = bf16[8,8,64,128]{3,1,2,0:T(8,128)(2,1)S(1)} async-done(((bf16[8,8,64,128]{3,1,2,0:T(8,128)(2,1)}), bf16[8,8,64,128]{3,1,2,0:T(8,128)(2,1)S(1)}, u32[]{:S(2)}, u32[]{:S(2)}) %all-to-all-start.1) | async-done | bytes 1048608 | tf_op jit(solution)/shard_map/all_to_all | solution.py:99
  292.2 0.3 fusion.3
  292.4 0.2 multiply_reduce_fusion
  292.7 0.7 fusion.13
  293.3 1.2 copy.20
  294.6 1.2 copy.21
  (13 shorter events, 0.1 us)
Async XLA Ops:
  7.2 259.2 %copy-start = (bf16[8,8,128]{2,1,0:T(8,128)(2,1)S(1)}, bf16[8,8,128]{2,1,0:T(8,128)(2,1)}, u32[]{:S(2)}) copy-start(bf16[8,8,128]{2,1,0:T(8,128)(2,1)} %param.13) | copy-start | bytes 49156
  7.2 119.2 %all-gather.4.cloned.1.call-start = ((), (), s32[]{:S(2)}) async-start(), calls=%async_computation.3 | async-start | bytes 8912896 | tf_op jit(solution)/shard_map/all_gather | solution.py:12
  7.9 244.3 %all-gather.6.cloned.1.call-start = ((), (), s32[]{:S(2)}) async-start(), calls=%async_computation.4 | async-start | bytes 8912896 | tf_op jit(solution)/shard_map/all_gather | solution.py:12
  90.6 46.3 %all-to-all-start.2 = ((f32[8,1,512]{2,1,0:T(1,128)}), f32[8,1,512]{2,1,0:T(1,128)S(1)}, u32[]{:S(2)}, u32[]{:S(2)}) async-start(f32[8,1,512]{2,1,0:T(1,128)} %reshape.81), calls=%async_computation.2 | async-start | bytes 32768 | tf_op jit(solution)/shard_map/all_to_all | solution.py:101
  136.9 125.8 %all-to-all-start = ((bf16[8,8,64,128]{3,1,2,0:T(8,128)(2,1)}), bf16[8,8,64,128]{3,1,2,0:T(8,128)(2,1)S(1)}, u32[]{:S(2)}, u32[]{:S(2)}) async-start(bf16[8,8,64,128]{3,1,2,0:T(8,128)(2,1)} %bitcast_bitcast_fusion.1), calls=%async_computation | async-start | bytes 2097152 | tf_op jit(solution)/shard_map/all_to_all | solution.py:98
  262.7 29.5 %all-to-all-start.1 = ((bf16[8,8,64,128]{3,1,2,0:T(8,128)(2,1)}), bf16[8,8,64,128]{3,1,2,0:T(8,128)(2,1)S(1)}, u32[]{:S(2)}, u32[]{:S(2)}) async-start(bf16[8,8,64,128]{3,1,2,0:T(8,128)(2,1)} %bitcast_bitcast_fusion), calls=%async_computation.1 | async-start | bytes 2097152 | tf_op jit(solution)/shard_map/all_to_all | solution.py:99
Sparse Core Ops, SparseCore 0:
  10.7 115.6 all-gather.3
  129.2 123.0 all-gather.5
where the time goes:
time: 303 us
  waiting for transfers between devices  168 us (55%)
  blocking collectives  75.4 us (25%)
  matrix products  22.4 us (7%)
  between operations  14.2 us (5%)
  starting transfers between devices  10.8 us (4%)
  local copies, waits for them, and re-layouts  7.45 us (2%)
  other arithmetic  3.86 us (1%)
    all_gather x2, waiting for transfers between devices, gathered(): return lax.all_gather(part, axis, axis=dim, tiled=True)  144 us
    all_gather x1, blocking collectives, gathered(): return lax.all_gather(part, axis, axis=dim, tiled=True)  44 us
    all_gather x1, blocking collectives, carried_in(): everything = jax.tree.map(lambda part: lax.all_gather(part, axis), array)  31.4 us
    all_to_all x1, waiting for transfers between devices, on_device(): lax.all_to_all(values, 'sp', split_axis=0, concat_axis=2, tiled=True)  22.9 us
    dot_general x3, matrix products, add_rows(): jnp.dot(columns, piece, preferred_element_type=jnp.float32)  21.7 us
  transfers between devices with their start and end apart: 5, of which 3 were waited for; matrix products, arithmetic and copies ran while one was open for 10% of the time, Pallas kernels for 0%

commit v1 on v0

--- a/solution.py
+++ b/solution.py
@@ -96,7 +96,10 @@
     cumulative = running_gate + earlier_sum[:, :, None]
     key_cache, value_cache = (
         lax.all_to_all(keys, "sp", split_axis=0, concat_axis=2, tiled=True),
-        lax.all_to_all(values, "sp", split_axis=0, concat_axis=2, tiled=True),
+        jnp.concatenate(
+            lax.all_to_all(jnp.stack(jnp.split(values, lax.axis_size("sp"), axis=0)), "sp", 0, 0),
+            axis=2,
+        ),
     )
     gate_cache = lax.all_to_all(cumulative, "sp", split_axis=0, concat_axis=2, tiled=True)
     member = lax.axis_index("sp")

time: 303 us -> 318 us (1.050)
  waiting for transfers between devices: 168 us -> 179 us
  local copies, waits for them, and re-layouts: 7.45 us -> 11.7 us
    all_to_all x1, waiting for transfers between devices: 0.01 us -> 20.5 us  [on_device(): lax.all_to_all(keys, 'sp', split_axis=0, concat_axis=2, tiled=True)]
    all_gather x2, waiting for transfers between devices: 144 us -> 135 us  [gathered(): return lax.all_gather(part, axis, axis=dim, tiled=True)]
    unnamed x6 -> x13, local copies, waits for them, and re-layouts: 1.31 us -> 5.91 us
  transfers between devices with their start and end apart: 5 -> 5, of which waited for: 3 -> 4; matrix products, arithmetic and copies ran while one was open for 10% -> 11% of each run, Pallas kernels for 0% -> 0%
where the time goes in v1:
time: 318 us; the launch traced here: 317 us
  waiting for transfers between devices  179 us (56%)
  blocking collectives  75.4 us (24%)
  matrix products  22.4 us (7%)
  between operations  14.2 us (4%)
  local copies, waits for them, and re-layouts  11.7 us (4%)
  starting transfers between devices  10.7 us (3%)
  other arithmetic  3.86 us (1%)
    all_gather x2, waiting for transfers between devices, gathered(): return lax.all_gather(part, axis, axis=dim, tiled=True)  135 us
    all_gather x1, blocking collectives, gathered(): return lax.all_gather(part, axis, axis=dim, tiled=True)  44 us
    all_gather x1, blocking collectives, carried_in(): everything = jax.tree.map(lambda part: lax.all_gather(part, axis), array)  31.4 us
    all_to_all x1, waiting for transfers between devices, on_device(): lax.all_to_all(jnp.stack(jnp.split(values, lax.axis_size('sp'), axis=0)),...  21.9 us
    dot_general x3, matrix products, add_rows(): jnp.dot(columns, piece, preferred_element_type=jnp.float32)  21.7 us
    all_to_all x1, waiting for transfers between devices, on_device(): lax.all_to_all(keys, 'sp', split_axis=0, concat_axis=2, tiled=True)  20.5 us
  transfers between devices with their start and end apart: 5, of which 4 were waited for; matrix products, arithmetic and copies ran while one was open for 11% of the time, Pallas kernels for 0%

profile of v1, /device:TPU:0, one launch (start us, length us, event | category | flops | bytes accessed | tf_op | source)
XLA Modules:
  0.0 317.5 jit_solution(9839570989811051629)
XLA Ops:
  7.2 0.0 copy-start
  7.2 0.0 all-gather.4.cloned.1.call-start
  7.2 0.7 all-gather.4.cloned.1.call-update
  7.9 0.0 all-gather.6.cloned.1.call-start
  8.0 0.7 all-gather.6.cloned.1.call-update
  8.7 44.0 %all_gather.14 = bf16[4096,8]{0,1:T(8,128)(2,1)S(1)} all-gather(bf16[256,8]{0,1:T(8,128)(2,1)} %param.11), channel_id=1, replica_groups=mesh['gr'=2,'sp'=8,'tp'=2] {'gr','sp'}, dimensions={0}, use_global_device_ids=true | all-gather | bytes 69632 | tf_op jit(solution)/shard_map/all_gather | solution.py:12
  52.7 3.4 %fusion.15 = f32[512,8]{0,1:T(8,128)S(1)} fusion(bf16[512,4096]{1,0:T(8,128)(2,1)} %bitcast.103, bf16[4096,8]{0,1:T(8,128)(2,1)S(1)} %all_gather.14, f32[8]{0:T(128)} %param.12), kind=kOutput, calls=%fused_computation.31 | convolution fusion | flops 33591296 | bytes 4276256 | tf_op jit(solution)/shard_map/dot_general | solution.py:66
  56.1 0.1 reshape.80
  56.2 1.8 reduce_window_sum.11
  57.9 0.1 slice.4
  58.0 0.1 copy.23
  58.1 31.4 %all-gather = f32[64,8,1]{1,2,0:T(1,128)S(1)} all-gather(f32[8,8,1]{1,2,0:T(1,128)S(1)} %copy.23), channel_id=2, replica_groups=mesh['gr'=2,'sp'=8,'tp'=2] {'sp'}, dimensions={0}, use_global_device_ids=true | all-gather | bytes 2304 | tf_op jit(solution)/shard_map/all_gather | solution.py:19
  89.6 0.2 while.14
  89.8 0.1 broadcast_add_fusion
  89.9 0.7 reshape.89
  90.6 3.3 %all-to-all-start.2 = ((f32[8,1,512]{2,1,0:T(1,128)}), f32[8,1,512]{2,1,0:T(1,128)S(1)}, u32[]{:S(2)}, u32[]{:S(2)}) async-start(f32[8,1,512]{2,1,0:T(1,128)} %reshape.89), calls=%async_computation.2 | async-start | bytes 32768 | tf_op jit(solution)/shard_map/all_to_all | solution.py:104
  93.9 32.5 %all-gather.4.cloned.1.call-done = bf16[4096,1024]{1,0:T(8,128)(2,1)} async-done(((bf16[256,1024]{1,0:T(8,128)(2,1)}), bf16[4096,1024]{1,0:T(8,128)(2,1)}) %all-gather.4.cloned.1.call-update) | async-done | bytes 8388624 | tf_op jit(solution)/shard_map/all_gather | solution.py:12
  126.4 9.1 %fusion = bf16[64,8,8,128]{3,1,2,0:T(8,128)(2,1)S(1)} fusion(bf16[512,4096]{1,0:T(8,128)(2,1)} %bitcast.104, bf16[4096,1024]{1,0:T(8,128)(2,1)} %all-gather.4.cloned.1.call-done), kind=kOutput, calls=%fused_computation.3 | convolution fusion | flops 4295491584 | bytes 13631488 | tf_op jit(solution)/shard_map/dot_general | solution.py:66
  135.6 0.3 copy.35
  135.8 1.0 bitcast_bitcast_fusion.1
  136.9 102.8 %all-gather.6.cloned.1.call-done = bf16[4096,1024]{1,0:T(8,128)(2,1)} async-done(((bf16[256,1024]{1,0:T(8,128)(2,1)}), bf16[4096,1024]{1,0:T(8,128)(2,1)}) %all-gather.6.cloned.1.call-update) | async-done | bytes 8388624 | tf_op jit(solution)/shard_map/all_gather | solution.py:12
  239.7 9.1 %fusion.1 = bf16[64,8,8,128]{3,1,2,0:T(8,128)(2,1)S(1)} fusion(bf16[512,4096]{1,0:T(8,128)(2,1)} %bitcast.105, bf16[4096,1024]{1,0:T(8,128)(2,1)} %all-gather.6.cloned.1.call-done), kind=kOutput, calls=%fused_computation.4 | convolution fusion | flops 4295491584 | bytes 13631488 | tf_op jit(solution)/shard_map/dot_general | solution.py:66
  248.9 0.3 copy.36
  249.1 0.1 bitcast_bitcast_fusion
  249.2 0.0 all-to-all-done.2
  249.2 3.7 %all-to-all-start = ((bf16[8,8,64,128]{3,1,2,0:T(8,128)(2,1)}), bf16[8,8,64,128]{3,1,2,0:T(8,128)(2,1)S(1)}, u32[]{:S(2)}, u32[]{:S(2)}) async-start(bf16[8,8,64,128]{3,1,2,0:T(8,128)(2,1)} %bitcast_bitcast_fusion.1), calls=%async_computation | async-start | bytes 2097152 | tf_op jit(solution)/shard_map/all_to_all | solution.py:98
  252.9 0.6 fusion.14
  253.6 0.7 fusion.13
  254.2 0.7 fusion.12
  254.9 0.7 fusion.11
  255.6 0.7 fusion.10
  256.2 0.6 fusion.9
  256.9 0.7 fusion.8
  257.5 0.7 fusion.7
  258.2 20.5 %all-to-all-done = bf16[8,8,64,128]{3,1,2,0:T(8,128)(2,1)S(1)} async-done(((bf16[8,8,64,128]{3,1,2,0:T(8,128)(2,1)}), bf16[8,8,64,128]{3,1,2,0:T(8,128)(2,1)S(1)}, u32[]{:S(2)}, u32[]{:S(2)}) %all-to-all-start) | async-done | bytes 1048608 | tf_op jit(solution)/shard_map/all_to_all | solution.py:98
  278.7 3.6 %all-to-all-start.1 = ((bf16[8,1,8,64,128]{4,2,3,1,0:T(8,128)(2,1)}), bf16[8,1,8,64,128]{4,2,3,1,0:T(8,128)(2,1)S(1)}, u32[]{:S(2)}, u32[]{:S(2)}) async-start(bf16[8,1,8,64,128]{4,2,3,1,0:T(8,128)(2,1)} %fusion.7), calls=%async_computation.1 | async-start | bytes 2097152 | tf_op jit(solution)/shard_map/all_to_all | solution.py:100
  282.3 0.0 copy-done
  282.3 0.5 broadcast.38
  282.8 0.7 reduce.6
  283.5 0.1 reshape.90
  283.6 0.1 all_to_all.40
  283.7 0.7 all_to_all.39
  284.4 1.2 copy.20
  285.6 0.4 fusion.5
  286.0 0.1 fusion.22
  286.1 0.2 fusion.18
  286.3 0.1 fusion.19
  286.4 21.9 %all-to-all-done.1 = bf16[8,1,8,64,128]{4,2,3,1,0:T(8,128)(2,1)S(1)} async-done(((bf16[8,1,8,64,128]{4,2,3,1,0:T(8,128)(2,1)}), bf16[8,1,8,64,128]{4,2,3,1,0:T(8,128)(2,1)S(1)}, u32[]{:S(2)}, u32[]{:S(2)}) %all-to-all-start.1) | async-done | bytes 1048608 | tf_op jit(solution)/shard_map/all_to_all | solution.py:100
  308.2 1.2 copy.21
  309.5 0.3 fusion.3
  309.8 0.2 multiply_reduce_fusion
  310.0 0.7 fusion.21
  (13 shorter events, 0.1 us)
Async XLA Ops:
  7.2 275.1 %copy-start = (bf16[8,8,128]{2,1,0:T(8,128)(2,1)S(1)}, bf16[8,8,128]{2,1,0:T(8,128)(2,1)}, u32[]{:S(2)}) copy-start(bf16[8,8,128]{2,1,0:T(8,128)(2,1)} %param.13) | copy-start | bytes 49156
  7.2 119.2 %all-gather.4.cloned.1.call-start = ((), (), s32[]{:S(2)}) async-start(), calls=%async_computation.3 | async-start | bytes 8912896 | tf_op jit(solution)/shard_map/all_gather | solution.py:12
  7.9 231.8 %all-gather.6.cloned.1.call-start = ((), (), s32[]{:S(2)}) async-start(), calls=%async_computation.4 | async-start | bytes 8912896 | tf_op jit(solution)/shard_map/all_gather | solution.py:12
  90.6 158.7 %all-to-all-start.2 = ((f32[8,1,512]{2,1,0:T(1,128)}), f32[8,1,512]{2,1,0:T(1,128)S(1)}, u32[]{:S(2)}, u32[]{:S(2)}) async-start(f32[8,1,512]{2,1,0:T(1,128)} %reshape.89), calls=%async_computation.2 | async-start | bytes 32768 | tf_op jit(solution)/shard_map/all_to_all | solution.py:104
  249.2 29.5 %all-to-all-start = ((bf16[8,8,64,128]{3,1,2,0:T(8,128)(2,1)}), bf16[8,8,64,128]{3,1,2,0:T(8,128)(2,1)S(1)}, u32[]{:S(2)}, u32[]{:S(2)}) async-start(bf16[8,8,64,128]{3,1,2,0:T(8,128)(2,1)} %bitcast_bitcast_fusion.1), calls=%async_computation | async-start | bytes 2097152 | tf_op jit(solution)/shard_map/all_to_all | solution.py:98
  278.7 29.5 %all-to-all-start.1 = ((bf16[8,1,8,64,128]{4,2,3,1,0:T(8,128)(2,1)}), bf16[8,1,8,64,128]{4,2,3,1,0:T(8,128)(2,1)S(1)}, u32[]{:S(2)}, u32[]{:S(2)}) async-start(bf16[8,1,8,64,128]{4,2,3,1,0:T(8,128)(2,1)} %fusion.7), calls=%async_computation.1 | async-start | bytes 2097152 | tf_op jit(solution)/shard_map/all_to_all | solution.py:100
Sparse Core Ops, SparseCore 0:
  10.7 115.6 all-gather.3
  129.2 110.5 all-gather.5
